TPU v7x, 256 devices: a whole 4x4x8 slice. The times are simulated.
256 devices in a mesh: ep: 64 (over z, x, core), tp: 4 (over y).
Axes of the slice: x: 4, y: 4, z: 8, core: 2. Of those that a mesh axis runs over, the one named last changes fastest.
Arguments:
- pool_in: bfloat16 [65536, 1024], P(('ep', 'tp')), may hold values from -6 to 6
- w_pool: bfloat16 [8, 128, 128], replicated, may hold values from -0.5 to 0.5
- pool_scale: float32 [1024], replicated, may hold values from 0.1 to 1.9
- w_out: bfloat16 [1024, 2048], replicated, may hold values from -0.1875 to 0.1875
- expert_in: bfloat16 [32768, 2048], P('ep'), may hold values from -6 to 6
- ffn_gain: float32 [2048], replicated, may hold values from 0.1 to 1.9
- routes: int32 [32768, 2], P('ep'), may hold values from 0 to 63, all different within a row; in each aligned block of 128 rows (0 to 127, 128 to 255, ...) at most 6 rows name the same one
- route_weight: float32 [32768, 2], P('ep'), may hold values from 0.25 to 1
- w_gate: bfloat16 [64, 2048, 1024], P('ep', None, 'tp'), may hold values from -0.125 to 0.125
- w_up: bfloat16 [64, 2048, 1024], P('ep', None, 'tp'), may hold values from -0.125 to 0.125
- w_down: bfloat16 [64, 1024, 2048], P('ep', 'tp'), may hold values from -0.1875 to 0.1875
Outputs:
- mixer_out: bfloat16 [65536, 2048], P(('ep', 'tp'))
- expert_out: bfloat16 [32768, 2048], P(('ep', 'tp'))
Inputs may be any that keep to these rules, and one draw needn't show every extreme that they name: `routes`: each row names 2 different experts. In each aligned block of 128 rows no expert is named by more than 6 rows, and in some block some expert is named by exactly 6 rows.
All inputs are finite; a program needn't handle non-finite values.
Results may differ from a plain program's by a relative error of at most 0.012.
Values may be sent and summed in bfloat16 or wider, within the bound.
No kernel may reach another device: no remote copies, remote signals or barrier semaphores. Data moves between devices by JAX's collectives and lax.ppermute only.
A program may use at most 128 MiB of HBM per device.

v0:
```python
from functools import partial
import jax
import jax.numpy as jnp
from jax import lax
from jax.sharding import PartitionSpec as P

GDIM = 128
WMAX = 16
K = 2
EPS = 0.05


def passed_along(array, axis, by):
    length = lax.axis_size(axis)
    pairs = [(i, i + by) for i in range(length) if 0 <= i + by < length]
    return lax.ppermute(array, axis, pairs)


def rows_first(arrays, axis, dims):
    turned = [jnp.moveaxis(a, dim, 0) for a, dim in zip(arrays, dims)]
    both = jnp.concatenate([t.reshape(len(t), -1) for t in turned], axis=1)
    out, at, gathered = (lax.all_gather(both, axis, axis=0, tiled=True), 0, [])
    for t, dim in zip(turned, dims):
        piece = out[:, at : at + t[0].size].reshape(-1, *t.shape[1:])
        gathered.append(jnp.moveaxis(piece, 0, dim))
        at += t[0].size
    return tuple(gathered)


def window_sizes(width):
    group_of = jnp.arange(width) // GDIM
    level = group_of % 4
    return jnp.where(
        level == 0, 2.0, jnp.where(level == 1, 4.0, jnp.where(level == 2, 8.0, 16.0))
    ).astype(jnp.float32)


def pooled_rows(extended, positions):
    extent = extended.shape[0] - (WMAX - 1)
    window = window_sizes(extended.shape[1])
    running = jnp.zeros((extent, extended.shape[1]), jnp.float32)
    picked = running
    for offset in range(WMAX):
        running = running + extended[WMAX - 1 - offset : WMAX - 1 - offset + extent]
        if offset + 1 in (2, 4, 8, 16):
            picked = jnp.where(window[None, :] == offset + 1, running, picked)
    counted = jnp.minimum(positions[:, None] + 1.0, window[None, :])
    return (picked / counted - extended[WMAX - 1 :]).astype(jnp.bfloat16)


def normalize(features_in, gain):
    features = features_in.astype(jnp.float32)
    inverse = lax.rsqrt(jnp.mean(features * features, axis=-1, keepdims=True) + EPS)
    return (features * inverse * gain).astype(jnp.bfloat16)


def slot_places(expert_ids, experts, capacity):
    onehot = (expert_ids[:, None] == jnp.arange(experts)[None, :]).astype(jnp.int32)
    earlier = jnp.cumsum(onehot, axis=0) - onehot
    slot_rank = jnp.sum(earlier * onehot, axis=1)
    return expert_ids * capacity + slot_rank


def send_block(normed_block, places, experts, capacity):
    pairs = places.shape[0]
    table = (
        jnp.full((experts * capacity,), pairs, jnp.int32)
        .at[places]
        .set(jnp.arange(pairs, dtype=jnp.int32))
    )
    source = jnp.where(table < pairs, table // K, normed_block.shape[0])
    padded = jnp.concatenate(
        [normed_block, jnp.zeros((1, normed_block.shape[1]), normed_block.dtype)], axis=0
    )
    return padded[source].reshape(experts, capacity, normed_block.shape[1])


def on_device(
    pool_in,
    w_pool,
    pool_scale,
    w_out,
    expert_in,
    ffn_gain,
    routes,
    route_weight,
    w_gate,
    w_up,
    w_down,
):
    rows_here = pool_in.shape[0]
    before = passed_along(pool_in[rows_here - (WMAX - 1) :], ("ep", "tp"), 1)
    extended = jnp.concatenate([before, pool_in], axis=0).astype(jnp.float32)
    positions = (lax.axis_index(("ep", "tp")) * rows_here + jnp.arange(rows_here)).astype(
        jnp.float32
    )
    pooled = pooled_rows(extended, positions)
    group_count = w_pool.shape[0]
    grouped = jnp.einsum(
        "tgc,gcd->tgd",
        pooled.reshape(rows_here, group_count, GDIM),
        w_pool,
        preferred_element_type=jnp.float32,
    )
    scaled = (grouped.reshape(rows_here, -1) * pool_scale).astype(jnp.bfloat16)
    mixer_out = jnp.dot(scaled, w_out, preferred_element_type=jnp.float32).astype(jnp.bfloat16)
    parts = lax.axis_size("tp")
    own = lax.axis_index("tp")
    experts = lax.axis_size("ep") * w_gate.shape[0]
    block_rows = routes.shape[0] // parts
    capacity = 3 * block_rows * K // (2 * experts)
    width = expert_in.shape[1]
    route_blocks = routes.reshape(parts, block_rows * K)
    weight_blocks = route_weight.reshape(parts, block_rows * K)
    places = jax.vmap(partial(slot_places, experts=experts, capacity=capacity))(route_blocks)
    gate_local = w_gate[0]
    up_local = w_up[0]
    down_local = w_down[0]
    gate_whole, up_whole, down_whole = rows_first(
        (gate_local, up_local, down_local), "tp", (1, 1, 0)
    )
    mine = lax.dynamic_slice_in_dim(expert_in, own * block_rows, block_rows, 0)
    own_places = lax.dynamic_index_in_dim(places, own, 0, keepdims=False)
    outgoing = send_block(normalize(mine, ffn_gain), own_places, experts, capacity)[None]
    arrived = lax.all_to_all(outgoing, "ep", split_axis=1, concat_axis=1, tiled=True)
    slot_rows = arrived.reshape(-1, width)
    gate_val = jnp.dot(slot_rows, gate_whole, preferred_element_type=jnp.float32)
    up_val = jnp.dot(slot_rows, up_whole, preferred_element_type=jnp.float32)
    hidden = (jax.nn.silu(gate_val) * up_val).astype(jnp.bfloat16)
    quarter = down_local.shape[0]
    total = jnp.zeros((slot_rows.shape[0], width), jnp.float32)
    for block in range(parts):
        partial_val = jnp.dot(
            hidden[:, block * quarter : (block + 1) * quarter],
            down_whole[block * quarter : (block + 1) * quarter],
            preferred_element_type=jnp.float32,
        ).astype(jnp.bfloat16)
        partial_val = lax.optimization_barrier(partial_val)
        total = total + partial_val.astype(jnp.float32)
    results = total.astype(jnp.bfloat16).reshape(experts, capacity, width)
    returned = lax.all_to_all(results, "ep", split_axis=0, concat_axis=0, tiled=True)
    mine_places = lax.dynamic_index_in_dim(places, own, 0, keepdims=False)
    mine_weights = lax.dynamic_index_in_dim(weight_blocks, own, 0, keepdims=False)
    values = returned.reshape(experts * capacity, width)[mine_places]
    weighted = values.astype(jnp.float32) * mine_weights[:, None]
    expert_out = jnp.sum(weighted.reshape(block_rows, K, width), axis=1).astype(jnp.bfloat16)
    return (mixer_out, expert_out)


def solution(mesh):
    placed = (
        P(("ep", "tp"), None),
        P(),
        P(),
        P(),
        P("ep", None),
        P(),
        P("ep", None),
        P("ep", None),
        P("ep", None, "tp"),
        P("ep", None, "tp"),
        P("ep", "tp", None),
    )
    return jax.shard_map(
        on_device,
        mesh=mesh,
        in_specs=placed,
        out_specs=(P(("ep", "tp"), None), P(("ep", "tp"), None)),
        check_vma=False,
    )
```

profile of v0, /device:TPU:96, one launch (start us, length us, event | category | flops | bytes accessed | tf_op | source)
XLA Modules:
  0.0 234.7 jit_solution(8038040765326191246)
XLA Ops:
  7.2 1.6 copy.36
  8.8 0.6 copy.35
  9.5 2.8 %pad_maximum_fusion = bf16[256,6144]{1,0:T(8,128)(2,1)} fusion(bf16[256,2048]{1,0:T(8,128)(2,1)} %bitcast.58, bf16[256,2048]{1,0:T(8,128)(2,1)S(1)} %bitcast.56, bf16[256,2048]{1,0:T(8,128)(2,1)S(1)} %bitcast.57), kind=kLoop, calls=%fused_computation.7 | loop fusion | flops 9437184 | bytes 6291456 | tf_op jit(solution)/shard_map/concatenate | solution.py:21
  12.4 0.6 copy-done.5
  13.2 0.2 eq.158
  13.5 2.4 %reduce-window.6 = s32[4,64,2,128]{3,1,2,0:T(8,128)S(1)} reduce-window(s32[4,64,2,128]{3,1,2,0:T(8,128)S(1)} %fusion.25, s32[]{:T(128)} %constant.95.clone.1), window={size=1x1x1x128 pad=0_0x0_0x0_0x127_0}, to_apply=%region_1.2 | reduce-window | flops 8323072 | bytes 524292 | tf_op jit(solution)/shard_map/reduce-window
  16.2 0.2 fusion.6
  16.5 0.2 fusion.8
  16.9 1.4 scatter_custom_fusion
  18.3 3.1 %gather_fusion = bf16[384,2048]{1,0:T(8,128)(2,1)} fusion(bf16[129,2048]{1,0:T(8,128)(2,1)S(1)} %concatenate.10, s32[1024]{0:T(1024)S(1)} %pad_clamp_fusion.1), kind=kCustom, calls=%fused_computation | custom fusion | bytes 3147264 | tf_op jit(solution)/shard_map/gather | solution.py:75
  21.4 2.5 %broadcast_in_dim_reshape.4 = bf16[1,64,6,2048]{3,2,1,0:T(8,128)(2,1)S(1)} reshape(bf16[384,2048]{1,0:T(8,128)(2,1)} %gather_fusion) | data formatting | bytes 3145728 | tf_op jit(solution)/shard_map/broadcast_in_dim;reshape | solution.py:124
  23.9 60.0 %all_to_all.10 = bf16[1,64,6,2048]{3,2,0,1:T(8,128)(2,1)} all-to-all(bf16[1,64,6,2048]{3,2,0,1:T(8,128)(2,1)S(1)} %bitcast.55), channel_id=1, replica_groups=mesh['ep'=64,'tp'=4] {'ep'}, dimensions={1} | all-to-all | bytes 3145728 | tf_op jit(solution)/shard_map/all_to_all | solution.py:125
  84.0 2.6 %reshape.143 = bf16[384,2048]{1,0:T(8,128)(2,1)S(1)} reshape(bf16[1,64,6,2048]{3,2,0,1:T(8,128)(2,1)} %all_to_all.10) | data formatting | bytes 3145728 | tf_op jit(solution)/shard_map/reshape | solution.py:126
  86.6 48.9 %all-gather.2.cloned.1.call-done = bf16[1024,6144]{1,0:T(8,128)(2,1)} async-done(((bf16[256,6144]{1,0:T(8,128)(2,1)}), bf16[1024,6144]{1,0:T(8,128)(2,1)}) %all-gather.2.cloned.1.call-update) | async-done | bytes 12582928 | tf_op jit(solution)/shard_map/all_gather | solution.py:22
  135.5 4.0 %fusion.2 = f32[384,1024]{1,0:T(8,128)S(1)} fusion(bf16[384,2048]{1,0:T(8,128)(2,1)S(1)} %reshape.143, bf16[1024,6144]{1,0:T(8,128)(2,1)} %all-gather.2.cloned.1.call-done), kind=kOutput, calls=%fused_computation.5 | convolution fusion | flops 1610612736 | bytes 7340032 | tf_op jit(solution)/shard_map/dot_general | solution.py:127
  139.5 4.1 %multiply_convert_fusion = bf16[384,1024]{1,0:T(8,128)(2,1)S(1)} fusion(f32[384,1024]{1,0:T(8,128)S(1)} %fusion.2, bf16[384,2048]{1,0:T(8,128)(2,1)S(1)} %reshape.143, bf16[1024,6144]{1,0:T(8,128)(2,1)} %all-gather.2.cloned.1.call-done), kind=kOutput, calls=%fused_computation.15 | convolution fusion | flops 1612972032 | bytes 8126464 | tf_op jit(solution)/shard_map/dot_general | solution.py:128
  143.6 1.8 convolution_convert_fusion.3
  145.4 1.8 convolution_convert_fusion.2
  147.2 1.8 convolution_convert_fusion.1
  149.0 1.8 convolution_convert_fusion
  150.8 1.2 add_convert_fusion
  152.1 1.6 reshape.144
  153.6 10.6 %all-to-all-start.1 = ((bf16[64,6,2048]{2,1,0:T(8,128)(2,1)}), bf16[64,6,2048]{2,1,0:T(8,128)(2,1)}, u32[]{:S(2)}, u32[]{:S(2)}) async-start(bf16[64,6,2048]{2,1,0:T(8,128)(2,1)} %reshape.144), calls=%async_computation.1 | async-start | bytes 4194304 | tf_op jit(solution)/shard_map/all_to_all | solution.py:141
  164.3 3.6 %collective-permute-start = (bf16[15,1024]{1,0:T(8,128)(2,1)S(1)}, bf16[15,1024]{1,0:T(8,128)(2,1)S(1)}, u32[]{:S(2)}, u32[]{:S(2)}) collective-permute-start(bf16[15,1024]{1,0:T(8,128)(2,1)S(1)} %slice.93), channel_id=1, source_target_pairs={{0,1},{1,2},{2,3},{3,4},{4,5},{5,6},{6,7},{7,8},{8,9},{9,10},{10,1... | collective-permute-start | bytes 92168 | tf_op jit(solution)/shard_map/ppermute | solution.py:16
  168.5 45.4 %collective-permute-done = bf16[15,1024]{1,0:T(8,128)(2,1)S(1)} collective-permute-done((bf16[15,1024]{1,0:T(8,128)(2,1)S(1)}, bf16[15,1024]{1,0:T(8,128)(2,1)S(1)}, u32[]{:S(2)}, u32[]{:S(2)}) %collective-permute-start) | collective-permute-done | bytes 30752 | tf_op jit(solution)/shard_map/ppermute | solution.py:16
  214.2 1.9 fusion.18
  216.1 0.2 fusion.16
  216.3 2.2 convolution_convert_fusion.4
  218.6 2.6 %reshape.145 = bf16[384,2048]{1,0:T(8,128)(2,1)S(1)} reshape(bf16[64,6,2048]{2,1,0:T(8,128)(2,1)} %all-to-all-done.1) | data formatting | bytes 3145728 | tf_op jit(solution)/shard_map/reshape | solution.py:144
  221.2 1.4 gather_fusion.1
  222.6 1.3 reshape.147
  223.9 3.9 %multiply_reduce_fusion = bf16[128,2048]{1,0:T(8,128)(2,1)} fusion(f32[128,2,2048]{2,1,0:T(2,128)S(1)} %reshape.147, f32[128,2]{1,0:T(8,128)S(1)} %mul.78), kind=kLoop, calls=%fused_computation.14 | loop fusion | flops 786432 | bytes 2622464 | tf_op jit(solution)/shard_map/reduce_sum | solution.py:146
  (46 shorter events, 1.7 us)
Async XLA Ops:
  7.2 207.0 %copy-start = (bf16[8,128,128]{2,1,0:T(8,128)(2,1)S(1)}, bf16[8,128,128]{2,1,0:T(8,128)(2,1)}, u32[]{:S(2)}) copy-start(bf16[8,128,128]{2,1,0:T(8,128)(2,1)} %param.12) | copy-start | bytes 786436
  7.2 1.6 copy-start.1
  7.2 128.3 %all-gather.2.cloned.1.call-start = ((), (), s32[]{:S(2)}) async-start(), calls=%async_computation.2 | async-start | bytes 15728640 | tf_op jit(solution)/shard_map/all_gather | solution.py:22
  12.3 0.7 copy-start.5
  12.3 3.9 %copy-start.3 = (bf16[512,2048]{1,0:T(8,128)(2,1)S(1)}, bf16[512,2048]{1,0:T(8,128)(2,1)}, u32[]{:S(2)}) copy-start(bf16[512,2048]{1,0:T(8,128)(2,1)} %param.15) | copy-start | bytes 6291460
  12.4 4.1 %copy-start.4 = (f32[2048]{0:T(1024)S(1)}, f32[2048]{0:T(1024)}, u32[]{:S(2)}) copy-start(f32[2048]{0:T(1024)} %param.16) | copy-start | bytes 24580
  153.6 10.7 %copy-start.2 = (bf16[256,1024]{1,0:T(8,128)(2,1)S(1)}, bf16[256,1024]{1,0:T(8,128)(2,1)}, u32[]{:S(2)}) copy-start(bf16[256,1024]{1,0:T(8,128)(2,1)} %param.11) | copy-start | bytes 1572868
  153.6 14.4 %copy-start.6 = (f32[512,2]{0,1:T(2,128)S(1)}, f32[512,2]{0,1:T(2,128)}, u32[]{:S(2)}) copy-start(f32[512,2]{0,1:T(2,128)} %param.18) | copy-start | bytes 12292
  153.6 65.0 %all-to-all-start.1 = ((bf16[64,6,2048]{2,1,0:T(8,128)(2,1)}), bf16[64,6,2048]{2,1,0:T(8,128)(2,1)}, u32[]{:S(2)}, u32[]{:S(2)}) async-start(bf16[64,6,2048]{2,1,0:T(8,128)(2,1)} %reshape.144), calls=%async_computation.1 | async-start | bytes 4194304 | tf_op jit(solution)/shard_map/all_to_all | solution.py:141
  164.3 49.7 %collective-permute-start = (bf16[15,1024]{1,0:T(8,128)(2,1)S(1)}, bf16[15,1024]{1,0:T(8,128)(2,1)S(1)}, u32[]{:S(2)}, u32[]{:S(2)}) collective-permute-start(bf16[15,1024]{1,0:T(8,128)(2,1)S(1)} %slice.93), channel_id=1, source_target_pairs={{0,1},{1,2},{2,3},{3,4},{4,5},{5,6},{6,7},{7,8},{8,9},{9,10},{10,1... | collective-permute-start | bytes 92168 | tf_op jit(solution)/shard_map/ppermute | solution.py:16
  214.1 2.0 copy-start.7
  214.1 2.2 copy-start.8
Sparse Core Ops, SparseCore 0:
  12.5 122.9 all-gather.1
where the time goes:
time: 235 us
  waiting for transfers between devices  94.4 us (40%)
  blocking collectives  60 us (26%)
  local copies, waits for them, and re-layouts  20.7 us (9%)
  matrix products  19.5 us (8%)
  between operations  14.4 us (6%)
  starting transfers between devices  14.3 us (6%)
  other arithmetic  11.4 us (5%)
    all_to_all x1, blocking collectives, on_device(): lax.all_to_all(outgoing, 'ep', split_axis=1, concat_axis=1, tiled=True)  60 us
    all_gather x1, waiting for transfers between devices, rows_first(): out, at, gathered = (lax.all_gather(both, axis, axis=0, tiled=True), 0, [])  48.9 us
    ppermute x1, waiting for transfers between devices, passed_along(): return lax.ppermute(array, axis, pairs)  45.4 us
    all_to_all x1, starting transfers between devices, on_device(): lax.all_to_all(results, 'ep', split_axis=0, concat_axis=0, tiled=True)  10.6 us
    dot_general x4, matrix products, on_device(): jnp.dot(hidden[:, block * quarter:(block + 1) * quarter], down_whole[bloc...  7.21 us
  transfers between devices with their start and end apart: 3, of which 2 were waited for; matrix products, arithmetic and copies ran while one was open for 8% of the time, Pallas kernels for 0%

commit v1 on v0

--- a/solution.py
+++ b/solution.py
@@ -3,6 +3,7 @@
 import jax.numpy as jnp
 from jax import lax
 from jax.sharding import PartitionSpec as P
+from jax.lax import all_to_all, axis_size
 
 GDIM = 128
 WMAX = 16
@@ -19,7 +20,19 @@
 def rows_first(arrays, axis, dims):
     turned = [jnp.moveaxis(a, dim, 0) for a, dim in zip(arrays, dims)]
     both = jnp.concatenate([t.reshape(len(t), -1) for t in turned], axis=1)
-    out, at, gathered = (lax.all_gather(both, axis, axis=0, tiled=True), 0, [])
+    out, at, gathered = (
+        jnp.concatenate(
+            all_to_all(
+                jnp.stack([both for _ in range(axis_size(axis))], axis=0),
+                axis_name=axis,
+                split_axis=0,
+                concat_axis=0,
+            ),
+            axis=0,
+        ),
+        0,
+        [],
+    )
     for t, dim in zip(turned, dims):
         piece = out[:, at : at + t[0].size].reshape(-1, *t.shape[1:])
         gathered.append(jnp.moveaxis(piece, 0, dim))

time: 235 us -> 314 us (1.34)
  waiting for transfers between devices: 94.4 us -> 225 us
  blocking collectives: 60 us -> 0 us
  starting transfers between devices: 14.3 us -> 28.9 us
  between operations: 14.4 us -> 1.03 us
  local copies, waits for them, and re-layouts: 20.7 us -> 26 us
    all_to_all x0 -> x2, waiting for transfers between devices: none -> 180 us  [the longest x1 135 us: rows_first(): all_to_all(jnp.stack([both for _ in range(axis_size(axis))], axis=0), axi...]
    all_to_all x1 -> x0, blocking collectives: 60 us -> none  [on_device(): lax.all_to_all(outgoing, 'ep', split_axis=1, concat_axis=1, tiled=True)]
    all_gather x1 -> x0, waiting for transfers between devices: 48.9 us -> none  [rows_first(): out, at, gathered = (lax.all_gather(both, axis, axis=0, tiled=True), 0, [])]
    all_to_all x0 -> x2, starting transfers between devices: none -> 17.6 us  [the longest x1 11 us: on_device(): lax.all_to_all(outgoing, 'ep', split_axis=1, concat_axis=1, tiled=True)]
    another operation x2 -> x3, local copies, waits for them, and re-layouts: 0.01 us -> 6.05 us  [the longest x1 6.04 us: rows_first(): jnp.stack([both for _ in range(axis_size(axis))], axis=0)]
  transfers between devices with their start and end apart: 3 -> 4, of which waited for: 2 -> 3; matrix products, arithmetic and copies ran while one was open for 8% -> 4% of each run, Pallas kernels for 0% -> 0%
where the time goes in v1:
time: 314 us; the launch traced here: 313 us
  waiting for transfers between devices  225 us (72%)
  starting transfers between devices  28.9 us (9%)
  local copies, waits for them, and re-layouts  26 us (8%)
  matrix products  19.5 us (6%)
  other arithmetic  12.6 us (4%)
    all_to_all x1, waiting for transfers between devices, rows_first(): all_to_all(jnp.stack([both for _ in range(axis_size(axis))], axis=0), axi...  135 us
    ppermute x1, waiting for transfers between devices, passed_along(): return lax.ppermute(array, axis, pairs)  45.6 us
    all_to_all x1, waiting for transfers between devices, on_device(): lax.all_to_all(outgoing, 'ep', split_axis=1, concat_axis=1, tiled=True)  44.4 us
    all_to_all x1, starting transfers between devices, on_device(): lax.all_to_all(outgoing, 'ep', split_axis=1, concat_axis=1, tiled=True)  11 us
    all_to_all x1, starting transfers between devices, on_device(): lax.all_to_all(results, 'ep', split_axis=0, concat_axis=0, tiled=True)  8.56 us
    dot_general x4, matrix products, on_device(): jnp.dot(hidden[:, block * quarter:(block + 1) * quarter], down_whole[bloc...  7.21 us
    all_to_all x1, starting transfers between devices, rows_first(): all_to_all(jnp.stack([both for _ in range(axis_size(axis))], axis=0), axi...  6.51 us
  transfers between devices with their start and end apart: 4, of which 3 were waited for; matrix products, arithmetic and copies ran while one was open for 4% of the time, Pallas kernels for 0%

profile of v1, /device:TPU:96, one launch (start us, length us, event | category | flops | bytes accessed | tf_op | source)
XLA Modules:
  0.0 313.3 jit_solution(11947091503206739326)
XLA Ops:
  1.9 1.2 fusion.6
  3.2 2.4 reduce-window.6
  6.0 1.4 scatter_custom_fusion
  7.5 1.2 fusion.8
  8.8 2.5 gather_fusion
  11.2 1.6 broadcast_in_dim_reshape.4
  12.9 11.0 %all-to-all-start = ((bf16[1,64,6,2048]{3,2,0,1:T(8,128)(2,1)}), bf16[1,64,6,2048]{3,2,0,1:T(8,128)(2,1)}, u32[]{:S(2)}, u32[]{:S(2)}) async-start(bf16[1,64,6,2048]{3,2,0,1:T(8,128)(2,1)} %bitcast.6), calls=%async_computation | async-start | bytes 4194304 | tf_op jit(solution)/shard_map/all_to_all | solution.py:138
  24.0 1.4 copy.36
  25.4 1.4 copy.35
  26.8 2.0 pad_maximum_fusion
  28.8 44.4 %all-to-all-done = bf16[1,64,6,2048]{3,2,0,1:T(8,128)(2,1)} async-done(((bf16[1,64,6,2048]{3,2,0,1:T(8,128)(2,1)}), bf16[1,64,6,2048]{3,2,0,1:T(8,128)(2,1)}, u32[]{:S(2)}, u32[]{:S(2)}) %all-to-all-start) | async-done | bytes 1572896 | tf_op jit(solution)/shard_map/all_to_all | solution.py:138
  73.3 6.0 %stack.2 = bf16[4,256,6144]{2,1,0:T(8,128)(2,1)} broadcast(bf16[256,6144]{1,0:T(8,128)(2,1)S(1)} %pad_maximum_fusion), dimensions={1,2} | broadcast | bytes 15728640 | tf_op jit(solution)/shard_map/stack | solution.py:26
  79.3 6.5 %all-to-all-start.1 = ((bf16[4,256,6144]{2,1,0:T(8,128)(2,1)}), bf16[4,256,6144]{2,1,0:T(8,128)(2,1)}, u32[]{:S(2)}, u32[]{:S(2)}) async-start(bf16[4,256,6144]{2,1,0:T(8,128)(2,1)} %stack.2), calls=%async_computation.1 | async-start | bytes 25165824 | tf_op jit(solution)/shard_map/all_to_all | solution.py:25
  85.8 2.6 reshape.148
  88.4 135.3 %all-to-all-done.1 = bf16[4,256,6144]{2,1,0:T(8,128)(2,1)} async-done(((bf16[4,256,6144]{2,1,0:T(8,128)(2,1)}), bf16[4,256,6144]{2,1,0:T(8,128)(2,1)}, u32[]{:S(2)}, u32[]{:S(2)}) %all-to-all-start.1) | async-done | bytes 12582944 | tf_op jit(solution)/shard_map/all_to_all | solution.py:25
  223.7 4.0 %fusion.2 = f32[384,1024]{1,0:T(8,128)S(1)} fusion(bf16[384,2048]{1,0:T(8,128)(2,1)S(1)} %reshape.148, bf16[1024,6144]{1,0:T(8,128)(2,1)} %bitcast.12), kind=kOutput, calls=%fused_computation.5 | convolution fusion | flops 1610612736 | bytes 7340032 | tf_op jit(solution)/shard_map/dot_general | solution.py:140
  227.7 4.1 %multiply_convert_fusion = bf16[384,1024]{1,0:T(8,128)(2,1)S(1)} fusion(f32[384,1024]{1,0:T(8,128)S(1)} %fusion.2, bf16[384,2048]{1,0:T(8,128)(2,1)S(1)} %reshape.148, bf16[1024,6144]{1,0:T(8,128)(2,1)} %bitcast.12), kind=kOutput, calls=%fused_computation.15 | convolution fusion | flops 1612972032 | bytes 8126464 | tf_op jit(solution)/shard_map/dot_general | solution.py:141
  231.9 1.8 convolution_convert_fusion
  233.7 1.8 convolution_convert_fusion.1
  235.5 1.8 convolution_convert_fusion.2
  237.3 1.8 convolution_convert_fusion.3
  239.1 1.2 add_convert_fusion
  240.3 1.6 reshape.150
  241.9 8.6 %all-to-all-start.2 = ((bf16[64,6,2048]{2,1,0:T(8,128)(2,1)}), bf16[64,6,2048]{2,1,0:T(8,128)(2,1)}, u32[]{:S(2)}, u32[]{:S(2)}) async-start(bf16[64,6,2048]{2,1,0:T(8,128)(2,1)} %reshape.150), calls=%async_computation.2 | async-start | bytes 4194304 | tf_op jit(solution)/shard_map/all_to_all | solution.py:154
  250.5 2.7 collective-permute-start
  253.8 45.6 %collective-permute-done = bf16[15,1024]{1,0:T(8,128)(2,1)S(1)} collective-permute-done((bf16[15,1024]{1,0:T(8,128)(2,1)S(1)}, bf16[15,1024]{1,0:T(8,128)(2,1)S(1)}, u32[]{:S(2)}, u32[]{:S(2)}) %collective-permute-start) | collective-permute-done | bytes 30752 | tf_op jit(solution)/shard_map/ppermute | solution.py:17
  299.6 1.9 fusion.18
  301.8 2.2 convolution_convert_fusion.4
  304.1 2.6 reshape.151
  306.7 1.4 gather_fusion.1
  308.1 1.3 reshape.153
  309.4 3.9 %multiply_reduce_fusion = bf16[128,2048]{1,0:T(8,128)(2,1)} fusion(f32[128,2,2048]{2,1,0:T(2,128)S(1)} %reshape.153, f32[128,2]{1,0:T(8,128)S(1)} %mul.78), kind=kLoop, calls=%fused_computation.14 | loop fusion | flops 786432 | bytes 2622464 | tf_op jit(solution)/shard_map/reduce_sum | solution.py:159
  (45 shorter events, 2.7 us)
Async XLA Ops:
  0.6 299.0 %copy-start = (bf16[8,128,128]{2,1,0:T(8,128)(2,1)S(1)}, bf16[8,128,128]{2,1,0:T(8,128)(2,1)}, u32[]{:S(2)}) copy-start(bf16[8,128,128]{2,1,0:T(8,128)(2,1)} %param.12) | copy-start | bytes 786436
  0.6 6.8 %copy-start.4 = (f32[2048]{0:T(1024)S(1)}, f32[2048]{0:T(1024)}, u32[]{:S(2)}) copy-start(f32[2048]{0:T(1024)} %param.16) | copy-start | bytes 24580
  12.9 11.1 %copy-start.1 = (bf16[1,2048,256]{2,1,0:T(8,128)(2,1)S(1)}, bf16[1,2048,256]{2,1,0:T(8,128)(2,1)}, u32[]{:S(2)}) copy-start(bf16[1,2048,256]{2,1,0:T(8,128)(2,1)} %param.20) | copy-start | bytes 3145732
  12.9 60.4 %all-to-all-start = ((bf16[1,64,6,2048]{3,2,0,1:T(8,128)(2,1)}), bf16[1,64,6,2048]{3,2,0,1:T(8,128)(2,1)}, u32[]{:S(2)}, u32[]{:S(2)}) async-start(bf16[1,64,6,2048]{3,2,0,1:T(8,128)(2,1)} %bitcast.6), calls=%async_computation | async-start | bytes 4194304 | tf_op jit(solution)/shard_map/all_to_all | solution.py:138
  23.9 1.4 copy-start.2
  79.3 144.4 %all-to-all-start.1 = ((bf16[4,256,6144]{2,1,0:T(8,128)(2,1)}), bf16[4,256,6144]{2,1,0:T(8,128)(2,1)}, u32[]{:S(2)}, u32[]{:S(2)}) async-start(bf16[4,256,6144]{2,1,0:T(8,128)(2,1)} %stack.2), calls=%async_computation.1 | async-start | bytes 25165824 | tf_op jit(solution)/shard_map/all_to_all | solution.py:25
  241.9 8.6 %copy-start.3 = (bf16[256,1024]{1,0:T(8,128)(2,1)S(1)}, bf16[256,1024]{1,0:T(8,128)(2,1)}, u32[]{:S(2)}) copy-start(bf16[256,1024]{1,0:T(8,128)(2,1)} %param.11) | copy-start | bytes 1572868
  241.9 11.4 %copy-start.5 = (f32[512,2]{0,1:T(2,128)S(1)}, f32[512,2]{0,1:T(2,128)}, u32[]{:S(2)}) copy-start(f32[512,2]{0,1:T(2,128)} %param.18) | copy-start | bytes 12292
  241.9 62.2 %all-to-all-start.2 = ((bf16[64,6,2048]{2,1,0:T(8,128)(2,1)}), bf16[64,6,2048]{2,1,0:T(8,128)(2,1)}, u32[]{:S(2)}, u32[]{:S(2)}) async-start(bf16[64,6,2048]{2,1,0:T(8,128)(2,1)} %reshape.150), calls=%async_computation.2 | async-start | bytes 4194304 | tf_op jit(solution)/shard_map/all_to_all | solution.py:154
  250.5 49.0 %collective-permute-start = (bf16[15,1024]{1,0:T(8,128)(2,1)S(1)}, bf16[15,1024]{1,0:T(8,128)(2,1)S(1)}, u32[]{:S(2)}, u32[]{:S(2)}) collective-permute-start(bf16[15,1024]{1,0:T(8,128)(2,1)S(1)} %slice.93), channel_id=1, source_target_pairs={{0,1},{1,2},{2,3},{3,4},{4,5},{5,6},{6,7},{7,8},{8,9},{9,10},{10,1... | collective-permute-start | bytes 92168 | tf_op jit(solution)/shard_map/ppermute | solution.py:17
  299.6 2.0 copy-start.6
  299.6 2.2 copy-start.7
